TPU v7x, 32 devices: a whole 2x2x4 slice. The times are simulated.
32 devices in a mesh: sp: 8 (over z, x), tp: 4 (over y, core).
Axes of the slice: x: 2, y: 2, z: 4, core: 2. Of those that a mesh axis runs over, the one named last changes fastest.
Arguments:
- hidden_rows: bfloat16 [1024, 2048], P('sp', 'tp'), may hold values from -6 to 6
- out_cot: bfloat16 [1024, 2048], P('sp', 'tp'), may hold values from -6 to 6
- routes: int32 [1024, 2], P('sp'), may hold values from 0 to 7, all different within a row; in each aligned block of 128 rows (0 to 127, 128 to 255, ...) at most 40 rows name the same one
- route_weight: float32 [1024, 2], P('sp'), may hold values from 0.2 to 2
- gate_w: bfloat16 [8, 2048, 1024], P('sp', None, 'tp'), may hold values from -0.125 to 0.125
- up_w: bfloat16 [8, 2048, 1024], P('sp', None, 'tp'), may hold values from -0.125 to 0.125
- down_w: bfloat16 [8, 1024, 2048], P('sp', 'tp'), may hold values from -0.1875 to 0.1875
- out_weight: bfloat16 [2048, 4096], P('sp', 'tp'), may hold values from -0.09375 to 0.09375
- step_inputs: bfloat16 [1024, 4096], P('sp', 'tp'), may hold values from -6 to 6
- input_map: bfloat16 [1024, 1024], P('sp', 'tp'), may hold values from -2 to 2
- output_map: bfloat16 [1024, 1024], P('sp', 'tp'), may hold values from -2 to 2
- log_decay: float32 [1024, 64], P('sp', 'tp'), may hold values from -1 to 0, as said below
- gate_z: bfloat16 [1024, 4096], P('sp', 'tp'), may hold values from -6 to 6
Outputs:
- grad_gate_w: float32 [8, 2048, 1024], P('sp', None, 'tp')
- grad_up_w: float32 [8, 2048, 1024], P('sp', None, 'tp')
- grad_down_w: float32 [8, 1024, 2048], P('sp', 'tp')
- grad_out_weight: float32 [2048, 4096], P('sp', 'tp')
- grad_step: bfloat16 [1024, 4096], P('sp', 'tp')
- grad_gate_z: bfloat16 [1024, 4096], P('sp', 'tp')
- grad_input_map: float32 [1024, 1024], P('sp', 'tp')
- grad_output_map: float32 [1024, 1024], P('sp', 'tp')
- grad_log_decay: float32 [1024, 64], P('sp', 'tp')
Inputs may be any that keep to these rules, and one draw needn't show every extreme that they name: `routes`: each row names 2 different experts. Among the positions of one index of sp no expert is named more than 40 times, a bound that some block reaches. `log_decay`: every entry is negative.
All inputs are finite; a program needn't handle non-finite values.
Results may differ from a plain program's by a relative error of at most 0.015.
Values may be sent and summed in bfloat16 or wider, within the bound.
A program may use at most 128 MiB of HBM per device.

v0:
```python
from functools import reduce
import jax
import jax.numpy as jnp
from jax import lax
from jax.sharding import PartitionSpec as P

D = 2048
HEAD_DIM = 64
NS = 128
BLOCK = 128
epsilon = 1e-06
exact_mode = lax.Precision.HIGHEST
by_rows = (((0,), (0,)), ((), ()))
by_cols = (((1,), (1,)), ((), ()))


def entering(part, axis, combine, identity, reverse):
    count = lax.axis_size(axis)
    place = lax.axis_index(axis)
    ahead = count - 1 - place if reverse else place
    gathered = jax.tree.map(lambda a: lax.all_gather(a, axis), part)
    state = jax.tree.map(lambda a, e: jnp.zeros_like(a) + jnp.asarray(e, a.dtype), part, identity)

    def one(hop, state):
        source = count - 1 - hop if reverse else hop
        return combine(
            state, jax.tree.map(lambda a: lax.dynamic_index_in_dim(a, source, 0, False), gathered)
        )

    return lax.fori_loop(0, ahead, one, state)


def block_step(carry_state, inputs):
    x_block, b_block, c_block, log_block = inputs
    per_group = x_block.shape[1] // b_block.shape[1]
    cum_log = jnp.cumsum(log_block, axis=0)
    token_places = jnp.arange(log_block.shape[0])
    lower_mask = (token_places[:, None] >= token_places[None, :])[:, :, None]
    log_spans = jnp.where(lower_mask, cum_log[:, None, :] - cum_log[None, :, :], 0.0)
    decay_mask = jnp.where(lower_mask, jnp.exp(log_spans), 0.0)
    scores = jnp.einsum("tgn,sgn->tsg", c_block, b_block, precision=exact_mode)
    scores = jnp.repeat(scores, per_group, axis=2)
    within = jnp.einsum("tsh,shp->thp", scores * decay_mask, x_block, precision=exact_mode)
    c_heads = jnp.repeat(c_block, per_group, axis=1)
    b_heads = jnp.repeat(b_block, per_group, axis=1)
    carried = (
        jnp.einsum("thn,hpn->thp", c_heads, carry_state, precision=exact_mode)
        * jnp.exp(cum_log)[:, :, None]
    )
    last_log = cum_log[-1]
    to_end = jnp.exp(last_log[None, :] - cum_log)
    new_state = carry_state * jnp.exp(last_log)[:, None, None] + jnp.einsum(
        "shn,shp->hpn", b_heads * to_end[:, :, None], x_block, precision=exact_mode
    )
    return (new_state, within + carried)


def mixer_forward(step_in, map_in, map_out, log_in, gate_in, entry_state):
    length, head_count = log_in.shape
    groups = map_in.shape[1] // NS
    blocks = length // BLOCK
    x_blocks = step_in.reshape(blocks, BLOCK, head_count, HEAD_DIM)
    b_blocks = map_in.reshape(blocks, BLOCK, groups, NS)
    c_blocks = map_out.reshape(blocks, BLOCK, groups, NS)
    log_blocks = log_in.reshape(blocks, BLOCK, head_count)
    _, outputs = lax.scan(block_step, entry_state, (x_blocks, b_blocks, c_blocks, log_blocks))
    mixed = outputs.reshape(length, head_count * HEAD_DIM)
    gated = (mixed * jax.nn.silu(gate_in)).reshape(length, groups, -1)
    normed = gated * lax.rsqrt(jnp.mean(gated * gated, axis=-1, keepdims=True) + epsilon)
    return normed.reshape(length, head_count * HEAD_DIM)


def segment_state(step_in, map_in, log_in):
    length, head_count = log_in.shape
    groups = map_in.shape[1] // NS
    cum_log = jnp.cumsum(log_in, axis=0)
    to_end = jnp.exp(cum_log[-1][None, :] - cum_log)
    b_heads = jnp.repeat(map_in.reshape(length, groups, NS), head_count // groups, axis=1)
    own_state = jnp.einsum(
        "shn,shp->hpn",
        b_heads * to_end[:, :, None],
        step_in.reshape(length, head_count, HEAD_DIM),
        precision=exact_mode,
    )
    return (jnp.exp(cum_log[-1]), own_state)


def compose_steps(earlier, later):
    return (earlier[0] * later[0], earlier[1] * later[0][:, None, None] + later[1])


def expert_backward(row_block, cot_block, gate_mat, up_mat, down_mat):
    gate_pre = jnp.dot(row_block, gate_mat, preferred_element_type=jnp.float32)
    up_pre = jnp.dot(row_block, up_mat, preferred_element_type=jnp.float32)
    gate_sigmoid = jax.nn.sigmoid(gate_pre)
    hidden = (gate_pre * gate_sigmoid * up_pre).astype(jnp.bfloat16)
    d_act = lax.dot_general(cot_block, down_mat, by_cols, preferred_element_type=jnp.float32)
    d_gate = (d_act * up_pre * gate_sigmoid * (1.0 + gate_pre * (1.0 - gate_sigmoid))).astype(
        jnp.bfloat16
    )
    d_up = (d_act * gate_pre * gate_sigmoid).astype(jnp.bfloat16)
    grad_down = lax.dot_general(hidden, cot_block, by_rows, preferred_element_type=jnp.float32)
    grad_gate = lax.dot_general(row_block, d_gate, by_rows, preferred_element_type=jnp.float32)
    grad_up = lax.dot_general(row_block, d_up, by_rows, preferred_element_type=jnp.float32)
    input_part = lax.dot_general(d_gate, gate_mat, by_cols, preferred_element_type=jnp.float32)
    input_part = input_part + lax.dot_general(
        d_up, up_mat, by_cols, preferred_element_type=jnp.float32
    )
    return (grad_gate, grad_up, grad_down, input_part)


def local(
    hidden_rows,
    out_cot,
    routes,
    route_weight,
    gate_w,
    up_w,
    down_w,
    out_weight,
    step_inputs,
    input_map,
    output_map,
    log_decay,
    gate_z,
):
    tok_rows, top_count = routes.shape
    local_experts = gate_w.shape[0]
    sp_devices = lax.axis_size("sp")
    total_experts = local_experts * sp_devices
    capacity = 5 * tok_rows * top_count // (4 * total_experts)
    flat_routes = routes.reshape(-1)
    expert_hits = (
        flat_routes[:, None] == jnp.arange(total_experts, dtype=jnp.int32)[None, :]
    ).astype(jnp.int32)
    slot_rank = jnp.sum((jnp.cumsum(expert_hits, axis=0) - expert_hits) * expert_hits, axis=1)
    target = (flat_routes * capacity + slot_rank).reshape(tok_rows, top_count)
    slot_ids = jnp.arange(total_experts * capacity, dtype=jnp.int32)[:, None]
    matches = [slot_ids == target[:, column][None, :] for column in range(top_count)]
    placing = reduce(jnp.logical_or, matches).astype(jnp.bfloat16)
    slot_weight = reduce(
        jnp.add,
        [
            jnp.sum(jnp.where(matches[column], route_weight[:, column][None, :], 0.0), axis=1)
            for column in range(top_count)
        ],
    )

    def place(source_rows):
        return jnp.dot(placing, source_rows, preferred_element_type=jnp.float32)

    sent_rows = place(hidden_rows).astype(jnp.bfloat16)
    sent_cot = (place(out_cot) * slot_weight[:, None]).astype(jnp.bfloat16)
    part_rows, part_cot = (
        lax.all_to_all(sent_rows, "sp", split_axis=0, concat_axis=0, tiled=True),
        lax.all_to_all(sent_cot, "sp", split_axis=0, concat_axis=0, tiled=True),
    )
    got_rows, got_cot = (
        lax.all_gather(part_rows, "tp", axis=1, tiled=True),
        lax.all_gather(part_cot, "tp", axis=1, tiled=True),
    )
    buffer_rows = sp_devices * capacity
    arranged_rows = (
        got_rows.reshape(sp_devices, local_experts, capacity, D)
        .transpose(1, 0, 2, 3)
        .reshape(local_experts, buffer_rows, D)
    )
    arranged_cot = (
        got_cot.reshape(sp_devices, local_experts, capacity, D)
        .transpose(1, 0, 2, 3)
        .reshape(local_experts, buffer_rows, D)
    )
    grad_gate, grad_up, grad_down, input_part = expert_backward(
        arranged_rows[0], arranged_cot[0], gate_w[0], up_w[0], down_w[0]
    )
    grads_gate = [grad_gate]
    grads_up = [grad_up]
    grads_down = [grad_down]
    partials = [input_part]
    stacked = (
        jnp.stack(partials)
        .reshape(local_experts, sp_devices, capacity, D)
        .transpose(1, 0, 2, 3)
        .reshape(-1, D)
    )
    summed = lax.psum_scatter(stacked.astype(jnp.bfloat16), "tp", scatter_dimension=1, tiled=True)
    returned = lax.all_to_all(summed, "sp", split_axis=0, concat_axis=0, tiled=True)
    routed = lax.dot_general(placing, returned, by_rows, preferred_element_type=jnp.float32)
    mid_part = (out_cot.astype(jnp.float32) + routed).astype(jnp.bfloat16)
    mid_grad = lax.all_gather(mid_part, "tp", axis=1, tiled=True)
    step_float = step_inputs.astype(jnp.float32)
    inmap_float = input_map.astype(jnp.float32)
    outmap_float = output_map.astype(jnp.float32)
    gates_float = gate_z.astype(jnp.float32)
    (decay_total, own_state), state_pullback = jax.vjp(
        segment_state, step_float, inmap_float, log_decay
    )
    identity = (jnp.ones_like(decay_total), jnp.zeros_like(own_state))
    _, entry_state = entering((decay_total, own_state), "sp", compose_steps, identity, False)
    normed, out_pullback = jax.vjp(
        mixer_forward, step_float, inmap_float, outmap_float, log_decay, gates_float, entry_state
    )
    normed_half = normed.astype(jnp.bfloat16)
    columns = mid_grad
    grad_out_weight = lax.psum_scatter(
        lax.dot_general(columns, normed_half, by_rows, preferred_element_type=jnp.float32),
        "sp",
        scatter_dimension=0,
        tiled=True,
    )
    columns = mid_grad
    d_normed = jnp.dot(
        columns,
        lax.all_gather(out_weight, "sp", axis=0, tiled=True),
        preferred_element_type=jnp.float32,
    )
    grad_step, grad_in_map, grad_out_map, grad_log, grad_gate, grad_entry = out_pullback(d_normed)
    _, carried_grad = entering((decay_total, grad_entry), "sp", compose_steps, identity, True)
    extra_step, extra_in_map, extra_log = state_pullback(
        (jnp.sum(carried_grad * entry_state, axis=(1, 2)), carried_grad)
    )
    return (
        jnp.stack(grads_gate),
        jnp.stack(grads_up),
        jnp.stack(grads_down),
        grad_out_weight,
        (grad_step + extra_step).astype(jnp.bfloat16),
        grad_gate.astype(jnp.bfloat16),
        grad_in_map + extra_in_map,
        grad_out_map,
        grad_log + extra_log,
    )


def solution(mesh):
    placed = (
        P("sp", "tp"),
        P("sp", "tp"),
        P("sp", None),
        P("sp", None),
        P("sp", None, "tp"),
        P("sp", None, "tp"),
        P("sp", "tp", None),
        P("sp", "tp"),
        P("sp", "tp"),
        P("sp", "tp"),
        P("sp", "tp"),
        P("sp", "tp"),
        P("sp", "tp"),
    )
    return jax.shard_map(
        local,
        mesh=mesh,
        in_specs=placed,
        out_specs=(
            P("sp", None, "tp"),
            P("sp", None, "tp"),
            P("sp", "tp", None),
            P("sp", "tp"),
            P("sp", "tp"),
            P("sp", "tp"),
            P("sp", "tp"),
            P("sp", "tp"),
            P("sp", "tp"),
        ),
        check_vma=False,
    )
```

profile of v0, /device:TPU:0, one launch (start us, length us, event | category | flops | bytes accessed | tf_op | source)
XLA Modules:
  0.0 479.5 jit_solution(6448955937463369872)
XLA Ops:
  11.1 1.1 convolution_convert_fusion
  12.3 18.1 %all_to_all.36 = bf16[8,40,512]{2,1,0:T(8,128)(2,1)} all-to-all(bf16[8,40,512]{2,1,0:T(8,128)(2,1)S(1)} %bitcast.223), channel_id=1, replica_groups=mesh['sp'=8,'tp'=4] {'sp'}, dimensions={0} | all-to-all | bytes 655360 | tf_op jit(solution)/shard_map/all_to_all | solution.py:155
  30.9 13.7 %all_to_all.37 = bf16[8,40,512]{2,1,0:T(8,128)(2,1)} all-to-all(bf16[8,40,512]{2,1,0:T(8,128)(2,1)S(1)} %bitcast.222), channel_id=1, replica_groups=mesh['sp'=8,'tp'=4] {'sp'}, dimensions={0} | all-to-all | bytes 655360 | tf_op jit(solution)/shard_map/all_to_all | solution.py:156
  44.7 2.4 all-gather.9.cloned.1.call-done
  47.2 1.9 fusion.15
  49.6 17.3 %all-gather.11.cloned.1.call-done = bf16[320,2048]{1,0:T(8,128)(2,1)} async-done(((bf16[320,512]{1,0:T(8,128)(2,1)}), bf16[320,2048]{1,0:T(8,128)(2,1)}) %all-gather.11.cloned.1.call-update) | async-done | bytes 1310736 | tf_op jit(solution)/shard_map/all_gather | solution.py:160
  66.9 2.2 multiply_convert_fusion.2
  69.8 1.6 fusion
  73.9 2.0 convolution_bitcast_fusion.7
  76.5 21.5 %reduce-scatter.3.cloned.1.call-done = bf16[320,512]{1,0:T(8,128)(2,1)} async-done(((bf16[320,2048]{1,0:T(8,128)(2,1)}), bf16[320,512]{1,0:T(8,128)(2,1)}) %reduce-scatter.3.cloned.1.call-update) | async-done | bytes 327696 | tf_op jit(solution)/shard_map/reduce_scatter | solution.py:186
  98.0 5.5 %all-to-all-start.2 = ((bf16[8,40,512]{2,1,0:T(8,128)(2,1)}), bf16[8,40,512]{2,1,0:T(8,128)(2,1)S(1)}, u32[]{:S(2)}, u32[]{:S(2)}) async-start(bf16[8,40,512]{2,1,0:T(8,128)(2,1)} %bitcast.227), calls=%async_computation.3 | async-start | bytes 655360 | tf_op jit(solution)/shard_map/all_to_all | solution.py:187
  105.0 1.3 bitcast_multiply_fusion.4
  106.3 21.9 %all-gather.2 = f32[8,1,16]{2,1,0:T(1,128)S(1)} all-gather(f32[1,1,16]{2,1,0:T(1,128)} %get-tuple-element.531), channel_id=1, replica_groups=mesh['sp'=8,'tp'=4] {'sp'}, dimensions={0}, use_global_device_ids=true | all-gather | bytes 576 | tf_op jit(solution)/shard_map/all_gather | solution.py:21
  129.7 7.0 %all_gather.32 = bf16[128,2048]{1,0:T(8,128)(2,1)} all-gather(bf16[128,512]{1,0:T(8,128)(2,1)S(1)} %fusion.4), channel_id=1, replica_groups=mesh['sp'=8,'tp'=4] {'tp'}, dimensions={1}, use_global_device_ids=true | all-gather | bytes 655360 | tf_op jit(solution)/shard_map/all_gather | solution.py:190
  136.7 12.8 %all-gather.15.cloned.1.call-done = f32[128,64,128]{2,1,0:T(8,128)} async-done(((f32[16,64,128]{2,1,0:T(8,128)}), f32[128,64,128]{2,1,0:T(8,128)}) %all-gather.15.cloned.1.call-update) | async-done | bytes 4194320 | tf_op jit(solution)/shard_map/all_gather | solution.py:21
  149.8 2.1 convolution_bitcast_fusion.6
  152.0 2.0 fusion.1
  154.0 1.2 copy.224
  155.2 66.9 %all-gather.13.cloned.1.call-done = bf16[2048,1024]{1,0:T(8,128)(2,1)} async-done(((bf16[256,1024]{1,0:T(8,128)(2,1)}), bf16[2048,1024]{1,0:T(8,128)(2,1)}) %all-gather.13.cloned.1.call-update) | async-done | bytes 4194320 | tf_op jit(solution)/shard_map/all_gather | solution.py:214
  222.2 4.3 fusion.68
  226.5 2.3 mul.373
  228.8 1.9 reduce_sum.232
  230.7 1.4 copy.225
  232.1 2.3 mul.379
  234.4 1.9 reduce_sum.233
  236.3 1.5 copy.228
  237.7 1.3 multiply_multiply_fusion
  239.0 1.4 copy.226
  242.3 1.4 copy.229
  243.8 1.1 broadcast_in_dim.186
  245.1 1.2 fusion.31
  246.3 1.2 copy.230
  247.5 3.1 convolution_add_fusion.2
  250.9 6.0 %fusion.39 = f32[2048,1024]{1,0:T(8,128)} fusion(bf16[128,2048]{1,0:T(8,128)(2,1)} %all_gather.32, f32[128,1024]{1,0:T(8,128)} %bitcast.211, f32[128,1024]{1,0:T(8,128)} %copy-done.3, bf16[128,1024]{1,0:T(8,128)(2,1)} %param.29), kind=kOutput, calls=%fused_computation.85 | convolution fusion | flops 537919488 | bytes 10223616 | tf_op jit(solution)/shard_map/dot_general | solution.py:206
  256.9 1.8 fusion.43
  258.7 2.1 convolution_bitcast_fusion.1
  260.8 2.1 convolution_bitcast_fusion.2
  262.9 2.1 convolution_bitcast_fusion
  265.7 1.4 copy.239
  267.1 2.6 bitcast_reduce_fusion.2
  269.7 1.3 fusion.25
  271.0 1.4 copy.240
  272.4 1.4 copy.241
  273.8 2.5 bitcast_reduce_fusion
  276.3 1.7 copy.237
  278.0 1.9 fusion.5
  279.9 1.7 copy.245
  281.6 3.2 convolution_add_fusion.3
  284.7 37.2 %all-gather.17.cloned.1.call-done = f32[128,64,128]{2,1,0:T(8,128)} async-done(((f32[16,64,128]{2,1,0:T(8,128)}), f32[128,64,128]{2,1,0:T(8,128)}) %all-gather.17.cloned.1.call-update) | async-done | bytes 4194320 | tf_op jit(solution)/shard_map/all_gather | solution.py:21
  322.0 13.6 %while.20 = (s32[]{:T(128)}, f32[16,64,128]{2,1,0:T(8,128)S(1)}, s32[]{:T(128)}, f32[8,16]{1,0:T(8,128)}, f32[8,16,64,128]{3,2,1,0:T(8,128)}, /*index=5*/s32[]{:T(128)}, s32[]{:T(128)}, s32[]{:T(128)}, s32[]{:T(128)}) while((s32[]{:T(128)}, f32[16,64,128]{2,1,0:T(8,128)S(1)}, s32[]{:T(128)}, f32[8,16]{1,0:T(8,128)}, ...), condition=%wide.region_13.14_spmd, body=%wide.region_12.13_spmd.sunk | while | flops 262150 | bytes 1573203 | solution.py:30
  322.7 1.2 bitcast_add_fusion.6
  324.6 1.2 bitcast_add_fusion.6
  326.5 1.2 bitcast_add_fusion.6
  328.4 1.2 bitcast_add_fusion.6
  330.3 1.2 bitcast_add_fusion.6
  332.2 1.2 bitcast_add_fusion.6
  334.2 1.2 bitcast_add_fusion.6
  336.6 1.3 bitcast_reduce_fusion.3
  339.6 1.1 pad_add_fusion
  340.7 1.1 reduce_window_sum.54
  341.8 1.1 reduce_window_sum.55
  343.6 1.3 fusion.7
  345.7 1.1 fusion.3
  347.6 124.5 %reduce-scatter.5.cloned.1.call-done = f32[256,1024]{1,0:T(8,128)} async-done(((f32[2048,1024]{1,0:T(8,128)}), f32[256,1024]{1,0:T(8,128)}) %reduce-scatter.5.cloned.1.call-update) | async-done | bytes 1048592 | tf_op jit(solution)/shard_map/reduce_scatter | solution.py:205
  (172 shorter events, 24.0 us)
Async XLA Ops:
  8.0 39.1 %copy-start = (bf16[1,2048,256]{2,1,0:T(8,128)(2,1)S(1)}, bf16[1,2048,256]{2,1,0:T(8,128)(2,1)}, u32[]{:S(2)}) copy-start(bf16[1,2048,256]{2,1,0:T(8,128)(2,1)} %param.21) | copy-start | bytes 3145732
  8.0 22.4 %copy-start.45 = (f32[128,2]{0,1:T(2,128)S(1)}, f32[128,2]{0,1:T(2,128)}, u32[]{:S(2)}) copy-start(f32[128,2]{0,1:T(2,128)} %param.20) | copy-start | bytes 3076
  8.0 22.6 %copy-start.29 = (bf16[128,512]{1,0:T(8,128)(2,1)S(1)}, bf16[128,512]{1,0:T(8,128)(2,1)}, u32[]{:S(2)}) copy-start(bf16[128,512]{1,0:T(8,128)(2,1)} %param.18) | copy-start | bytes 393220
  8.0 39.1 %all-gather.9.cloned.1.call-start = ((), (), s32[]{:S(2)}) async-start(), calls=%async_computation.5 | async-start | bytes 1638400 | tf_op jit(solution)/shard_map/all_gather | solution.py:159
  11.1 33.5 %copy-start.41 = (s32[128]{0:T(128)}, s32[128]{0:T(128)S(1)}, u32[]{:S(2)}) copy-start(s32[128]{0:T(128)S(1)} %get-tuple-element.536) | copy-start | bytes 1540
  11.1 33.5 %copy-start.42 = (s32[128]{0:T(128)}, s32[128]{0:T(128)S(1)}, u32[]{:S(2)}) copy-start(s32[128]{0:T(128)S(1)} %get-tuple-element.537) | copy-start | bytes 1540
  30.4 36.5 %all-gather.11.cloned.1.call-start = ((), (), s32[]{:S(2)}) async-start(), calls=%async_computation.6 | async-start | bytes 1638400 | tf_op jit(solution)/shard_map/all_gather | solution.py:160
  44.7 4.4 copy-start.17
  44.7 53.3 %reduce-scatter.3.cloned.1.call-start = ((), (), s32[]{:S(2)}) async-start(), calls=%async_computation.7 | async-start | bytes 1638400 | tf_op jit(solution)/shard_map/reduce_scatter | solution.py:186
  47.1 1.9 copy-start.4
  49.1 17.8 %copy-start.30 = (f32[320,256]{1,0:T(8,128)}, f32[320,256]{1,0:T(8,128)S(1)}, u32[]{:S(2)}) copy-start(f32[320,256]{1,0:T(8,128)S(1)} %fusion.15) | copy-start | bytes 983044
  49.6 19.5 %copy-start.32 = (f32[320,256]{1,0:T(8,128)}, f32[320,256]{1,0:T(8,128)S(1)}, u32[]{:S(2)}) copy-start(f32[320,256]{1,0:T(8,128)S(1)} %fusion.18) | copy-start | bytes 983044
  69.1 0.7 copy-start.23
  69.1 0.7 copy-start.21
  71.4 0.7 copy-start.43
  71.4 1.6 copy-start.39
  71.4 2.2 copy-start.34
  71.5 78.0 %all-gather.15.cloned.1.call-start = ((), (), s32[]{:S(2)}) async-start(), calls=%async_computation.10 | async-start | bytes 4718592 | tf_op jit(solution)/shard_map/all_gather | solution.py:21
  72.4 55.8 %copy-start.15 = (f32[128,16]{1,0:T(8,128)}, f32[128,16]{1,0:T(8,128)S(1)}, u32[]{:S(2)}) copy-start(f32[128,16]{1,0:T(8,128)S(1)} %reduce_window_sum.53) | copy-start | bytes 24580
  73.0 0.6 copy-start.18
  73.0 2.8 copy-start.37
  75.9 27.7 %copy-start.40 = (bf16[128,256]{1,0:T(8,128)(2,1)S(1)}, bf16[128,256]{1,0:T(8,128)(2,1)}, u32[]{:S(2)}) copy-start(bf16[128,256]{1,0:T(8,128)(2,1)} %param.27) | copy-start | bytes 196612
  75.9 146.3 %all-gather.13.cloned.1.call-start = ((), (), s32[]{:S(2)}) async-start(), calls=%async_computation.9 | async-start | bytes 4718592 | tf_op jit(solution)/shard_map/all_gather | solution.py:214
  98.0 30.8 %all-to-all-start.2 = ((bf16[8,40,512]{2,1,0:T(8,128)(2,1)}), bf16[8,40,512]{2,1,0:T(8,128)(2,1)S(1)}, u32[]{:S(2)}, u32[]{:S(2)}) async-start(bf16[8,40,512]{2,1,0:T(8,128)(2,1)} %bitcast.227), calls=%async_computation.3 | async-start | bytes 655360 | tf_op jit(solution)/shard_map/all_to_all | solution.py:187
  103.5 218.4 %all-gather.17.cloned.1.call-start = ((), (), s32[]{:S(2)}) async-start(), calls=%async_computation.11 | async-start | bytes 4718592 | tf_op jit(solution)/shard_map/all_gather | solution.py:21
  103.8 32.9 %copy-start.25 = (bf16[128,2,128]{0,2,1:T(8,128)(2,1)}, bf16[128,2,128]{0,2,1:T(8,128)(2,1)S(1)}, u32[]{:S(2)}) copy-start(bf16[128,2,128]{0,2,1:T(8,128)(2,1)S(1)} %copy.234) | copy-start | bytes 196612
  103.9 0.6 copy-start.26
  104.9 44.6 %copy-start.13 = (f32[128,128,2]{1,0,2:T(8,128)}, f32[128,128,2]{1,0,2:T(8,128)S(1)}, u32[]{:S(2)}) copy-start(f32[128,128,2]{1,0,2:T(8,128)S(1)} %copy.214) | copy-start | bytes 393220
  105.0 23.8 %copy-start.35 = (pred[128,128]{1,0:T(8,128)(4,1)}, pred[128,128]{1,0:T(8,128)(4,1)S(1)}, u32[]{:S(2)}) copy-start(pred[128,128]{1,0:T(8,128)(4,1)S(1)} %iota_compare_fusion.2) | copy-start | bytes 49156
  149.7 2.3 copy-start.44
  149.8 4.2 copy-start.1
  149.8 2.2 copy-start.2
  152.0 2.0 copy-start.7
  155.2 89.8 %copy-start.3 = (f32[128,1024]{1,0:T(8,128)}, f32[128,1024]{1,0:T(8,128)S(1)}, u32[]{:S(2)}) copy-start(f32[128,1024]{1,0:T(8,128)S(1)} %copy.224) | copy-start | bytes 1572868
  243.8 1.3 copy-start.6
  243.8 1.3 copy-start.9
  243.8 1.3 copy-start.11
  250.6 221.5 %reduce-scatter.5.cloned.1.call-start = ((), (), s32[]{:S(2)}) async-start(), calls=%async_computation.8 | async-start | bytes 9437184 | tf_op jit(solution)/shard_map/reduce_scatter | solution.py:205
  256.9 1.8 copy-start.5
  256.9 1.8 copy-start.22
  258.7 2.1 copy-start.24
  260.8 2.1 copy-start.12
  260.8 2.1 copy-start.31
  260.8 2.1 copy-start.33
  262.9 2.1 copy-start.8
  267.1 2.6 copy-start.14
  267.1 2.6 copy-start.36
  335.6 1.0 copy-start.38
  337.9 0.8 copy-start.19
  338.1 1.5 copy-start.16
  338.1 1.5 copy-start.20
  338.2 0.6 copy-start.27
  338.8 0.6 copy-start.28
  339.6 6.1 %copy-start.10 = (f32[16,64,128]{2,1,0:T(8,128)S(1)}, f32[16,64,128]{2,1,0:T(8,128)}, u32[]{:S(2)}) copy-start(f32[16,64,128]{2,1,0:T(8,128)} %convolution_add_fusion.3) | copy-start | bytes 1572868
Sparse Core Ops, SparseCore 0:
  30.5 16.5 all-gather.8
  48.7 18.1 all-gather.10
  71.6 26.3 reduce-scatter.2
Sparse Core Ops, SparseCore 1:
  76.0 73.4 all-gather.14
  151.5 70.7 all-gather.12
  250.7 71.1 all-gather.16
  326.1 145.9 reduce-scatter.4
where the time goes:
time: 481 us; the launch traced here: 479 us
  waiting for transfers between devices  283 us (59%)
  blocking collectives  60.6 us (13%)
  matrix products  51.6 us (11%)
  local copies, waits for them, and re-layouts  37.1 us (8%)
  other arithmetic  24.1 us (5%)
  between operations  16.1 us (3%)
  starting transfers between devices  6.02 us (1%)
    reduce_scatter x1, waiting for transfers between devices, local(): lax.psum_scatter(lax.dot_general(columns, normed_half, by_rows, preferred...  125 us
    all_gather x1, waiting for transfers between devices, local(): lax.all_gather(out_weight, 'sp', axis=0, tiled=True)  66.9 us
    all_gather x2, waiting for transfers between devices, entering(): gathered = jax.tree.map(lambda a: lax.all_gather(a, axis), part)  50 us
    all_gather x1, blocking collectives, entering(): gathered = jax.tree.map(lambda a: lax.all_gather(a, axis), part)  21.9 us
    reduce_scatter x1, waiting for transfers between devices, local(): lax.psum_scatter(stacked.astype(jnp.bfloat16), 'tp', scatter_dimension=1,...  21.5 us
    all_to_all x1, blocking collectives, local(): lax.all_to_all(sent_rows, 'sp', split_axis=0, concat_axis=0, tiled=True)  18.1 us
    all_gather x1, waiting for transfers between devices, local(): lax.all_gather(part_cot, 'tp', axis=1, tiled=True)  17.3 us
    all_to_all x1, blocking collectives, local(): lax.all_to_all(sent_cot, 'sp', split_axis=0, concat_axis=0, tiled=True)  13.7 us
  transfers between devices with their start and end apart: 8, of which 7 were waited for; matrix products, arithmetic and copies ran while one was open for 15% of the time, Pallas kernels for 0%

commit v1 on v0

--- a/solution.py
+++ b/solution.py
@@ -12,6 +12,11 @@
 exact_mode = lax.Precision.HIGHEST
 by_rows = (((0,), (0,)), ((), ()))
 by_cols = (((1,), (1,)), ((), ()))
+
+
+def gather_over(block, name, dim):
+    repeated = jnp.stack([block] * lax.axis_size(name))
+    return jnp.concatenate(lax.all_to_all(repeated, name, 0, 0), axis=dim)
 
 
 def entering(part, axis, combine, identity, reverse):
@@ -210,9 +215,7 @@
     )
     columns = mid_grad
     d_normed = jnp.dot(
-        columns,
-        lax.all_gather(out_weight, "sp", axis=0, tiled=True),
-        preferred_element_type=jnp.float32,
+        columns, gather_over(out_weight, "sp", 0), preferred_element_type=jnp.float32
     )
     grad_step, grad_in_map, grad_out_map, grad_log, grad_gate, grad_entry = out_pullback(d_normed)
     _, carried_grad = entering((decay_total, grad_entry), "sp", compose_steps, identity, True)

time: 481 us -> 526 us (1.094)
  blocking collectives: 60.6 us -> 132 us
  waiting for transfers between devices: 283 us -> 244 us
  local copies, waits for them, and re-layouts: 37.1 us -> 44.6 us
    all_gather x1, blocking collectives: 21.9 us -> 93.3 us  [entering(): gathered = jax.tree.map(lambda a: lax.all_gather(a, axis), part)]
    all_gather x1 -> x0, waiting for transfers between devices: 66.9 us -> none  [local(): lax.all_gather(out_weight, 'sp', axis=0, tiled=True)]
    all_gather x2, waiting for transfers between devices: 50 us -> 66.4 us  [entering(): gathered = jax.tree.map(lambda a: lax.all_gather(a, axis), part)]
    all_to_all x1, waiting for transfers between devices: 0.01 us -> 16.5 us  [local(): lax.all_to_all(summed, 'sp', split_axis=0, concat_axis=0, tiled=True)]
    mul x4 -> x0, local copies, waits for them, and re-layouts: 6.82 us -> none  [the longest x2 3.31 us: mixer_forward(): gated * lax.rsqrt(jnp.mean(gated * gated, axis=-1, keepdims=True) + epsilon)]
    dot_general x0 -> x1, local copies, waits for them, and re-layouts: none -> 6.52 us  [local(): jnp.dot(columns, gather_over(out_weight, 'sp', 0), preferred_element_type...]
    all_to_all x0 -> x1, local copies, waits for them, and re-layouts: none -> 6.5 us  [gather_over(): return jnp.concatenate(lax.all_to_all(repeated, name, 0, 0), axis=dim)]
    unnamed x101 -> x112, local copies, waits for them, and re-layouts: 9.05 us -> 13.6 us
  transfers between devices with their start and end apart: 8 -> 8, of which waited for: 7 -> 6; matrix products, arithmetic and copies ran while one was open for 15% -> 16% of each run, Pallas kernels for 0% -> 0%
where the time goes in v1:
time: 526 us; the launch traced here: 524 us
  waiting for transfers between devices  244 us (46%)
  blocking collectives  132 us (25%)
  matrix products  49.1 us (9%)
  local copies, waits for them, and re-layouts  44.6 us (8%)
  other arithmetic  27 us (5%)
  between operations  16 us (3%)
  starting transfers between devices  10.7 us (2%)
    reduce_scatter x1, waiting for transfers between devices, local(): lax.psum_scatter(lax.dot_general(columns, normed_half, by_rows, preferred...  120 us
    all_gather x1, blocking collectives, entering(): gathered = jax.tree.map(lambda a: lax.all_gather(a, axis), part)  93.3 us
    all_gather x2, waiting for transfers between devices, entering(): gathered = jax.tree.map(lambda a: lax.all_gather(a, axis), part)  66.4 us
    reduce_scatter x1, waiting for transfers between devices, local(): lax.psum_scatter(stacked.astype(jnp.bfloat16), 'tp', scatter_dimension=1,...  23.3 us
    all_to_all x1, blocking collectives, local(): lax.all_to_all(sent_rows, 'sp', split_axis=0, concat_axis=0, tiled=True)  18.1 us
    all_gather x1, waiting for transfers between devices, local(): lax.all_gather(part_cot, 'tp', axis=1, tiled=True)  17.3 us
    all_to_all x1, waiting for transfers between devices, local(): lax.all_to_all(summed, 'sp', split_axis=0, concat_axis=0, tiled=True)  16.5 us
    all_to_all x1, blocking collectives, local(): lax.all_to_all(sent_cot, 'sp', split_axis=0, concat_axis=0, tiled=True)  13.7 us
  transfers between devices with their start and end apart: 8, of which 6 were waited for; matrix products, arithmetic and copies ran while one was open for 16% of the time, Pallas kernels for 0%

profile of v1, /device:TPU:0, one launch (start us, length us, event | category | flops | bytes accessed | tf_op | source)
XLA Modules:
  0.0 523.9 jit_solution(12927801929527140490)
XLA Ops:
  8.1 0.9 copy.233
  11.1 1.1 convolution_convert_fusion
  12.2 18.1 %all_to_all.41 = bf16[8,40,512]{2,1,0:T(8,128)(2,1)} all-to-all(bf16[8,40,512]{2,1,0:T(8,128)(2,1)S(1)} %bitcast.242), channel_id=1, replica_groups=mesh['sp'=8,'tp'=4] {'sp'}, dimensions={0} | all-to-all | bytes 655360 | tf_op jit(solution)/shard_map/all_to_all | solution.py:160
  31.4 1.1 fusion.2
  32.5 13.7 %all_to_all.42 = bf16[8,40,512]{2,1,0:T(8,128)(2,1)} all-to-all(bf16[8,40,512]{2,1,0:T(8,128)(2,1)S(1)} %bitcast.241), channel_id=1, replica_groups=mesh['sp'=8,'tp'=4] {'sp'}, dimensions={0} | all-to-all | bytes 655360 | tf_op jit(solution)/shard_map/all_to_all | solution.py:161
  47.1 1.9 fusion.15
  49.6 17.3 %all-gather.10.cloned.1.call-done = bf16[320,2048]{1,0:T(8,128)(2,1)} async-done(((bf16[320,512]{1,0:T(8,128)(2,1)}), bf16[320,2048]{1,0:T(8,128)(2,1)}) %all-gather.10.cloned.1.call-update) | async-done | bytes 1310736 | tf_op jit(solution)/shard_map/all_gather | solution.py:165
  66.9 2.2 multiply_convert_fusion.1
  70.3 1.6 fusion
  73.2 2.0 convolution_bitcast_fusion.7
  75.2 23.3 %reduce-scatter.3.cloned.1.call-done = bf16[320,512]{1,0:T(8,128)(2,1)} async-done(((bf16[320,2048]{1,0:T(8,128)(2,1)}), bf16[320,512]{1,0:T(8,128)(2,1)}) %reduce-scatter.3.cloned.1.call-update) | async-done | bytes 327696 | tf_op jit(solution)/shard_map/reduce_scatter | solution.py:191
  98.5 5.5 %all-to-all-start.2 = ((bf16[8,40,512]{2,1,0:T(8,128)(2,1)}), bf16[8,40,512]{2,1,0:T(8,128)(2,1)S(1)}, u32[]{:S(2)}, u32[]{:S(2)}) async-start(bf16[8,40,512]{2,1,0:T(8,128)(2,1)} %bitcast.246), calls=%async_computation.3 | async-start | bytes 655360 | tf_op jit(solution)/shard_map/all_to_all | solution.py:192
  104.3 16.5 %all-to-all-done.2 = bf16[8,40,512]{2,1,0:T(8,128)(2,1)S(1)} async-done(((bf16[8,40,512]{2,1,0:T(8,128)(2,1)}), bf16[8,40,512]{2,1,0:T(8,128)(2,1)S(1)}, u32[]{:S(2)}, u32[]{:S(2)}) %all-to-all-start.2) | async-done | bytes 327712 | tf_op jit(solution)/shard_map/all_to_all | solution.py:192
  120.7 2.2 stack.11
  123.0 4.7 all-to-all-start.3
  129.7 0.9 copy.248
  130.6 1.4 bitcast_multiply_fusion.4
  132.0 93.3 %all-gather.2 = f32[8,1,16]{2,1,0:T(1,128)S(1)} all-gather(f32[1,1,16]{2,1,0:T(1,128)S(1)} %get-tuple-element.531), channel_id=1, replica_groups=mesh['sp'=8,'tp'=4] {'sp'}, dimensions={0}, use_global_device_ids=true | all-gather | bytes 576 | tf_op jit(solution)/shard_map/all_gather | solution.py:26
  226.1 6.6 %all_gather.29 = bf16[128,2048]{1,0:T(8,128)(2,1)S(1)} all-gather(bf16[128,512]{1,0:T(8,128)(2,1)S(1)} %fusion.4), channel_id=1, replica_groups=mesh['sp'=8,'tp'=4] {'tp'}, dimensions={1}, use_global_device_ids=true | all-gather | bytes 655360 | tf_op jit(solution)/shard_map/all_gather | solution.py:195
  233.5 1.1 broadcast_in_dim.183
  234.6 2.1 convolution_bitcast_fusion.6
  236.8 1.2 fusion.1
  238.8 1.5 multiply_reduce_fusion.4
  240.3 2.0 copy.255
  242.4 6.5 %copy.252 = bf16[8,256,1024]{2,1,0:T(8,128)(2,1)} copy(bf16[8,256,1024]{1,2,0:T(8,128)(2,1)} %all-to-all-done.3) | data formatting | bytes 8388608 | tf_op jit(solution)/shard_map/all_to_all | solution.py:19
  248.9 6.5 %copy.253 = bf16[1024,2048]{1,0:T(8,128)(2,1)} copy(bf16[1024,2048]{0,1:T(8,128)(2,1)} %bitcast.223) | data formatting | bytes 8388608 | tf_op jit(solution)/shard_map/dot_general | solution.py:217
  255.4 4.0 multiply_reduce_fusion.3
  260.1 1.0 copy.256
  261.1 2.1 multiply_reduce_fusion.1
  263.2 2.4 convolution_add_fusion.2
  265.9 1.1 fusion.39
  267.0 5.6 %fusion.69 = f32[2048,1024]{1,0:T(8,128)} fusion(bf16[128,2048]{1,0:T(8,128)(2,1)} %copy-done.4, bf16[128,1024]{0,1:T(8,128)(2,1)S(1)} %fusion.39), kind=kOutput, calls=%fused_computation.144 | convolution fusion | flops 536870912 | bytes 9175040 | tf_op jit(solution)/shard_map/dot_general | solution.py:211
  272.6 1.8 fusion.45
  274.4 2.1 convolution_bitcast_fusion.1
  276.5 2.1 convolution_bitcast_fusion.2
  278.6 2.1 convolution_bitcast_fusion
  280.7 1.8 bitcast_reduce_fusion.2
  285.4 2.5 bitcast_reduce_fusion
  287.8 1.7 copy.262
  289.5 1.9 fusion.5
  291.4 1.7 copy.271
  293.1 2.2 fusion.31
  295.3 1.8 copy.269
  297.1 2.9 convolution_add_fusion.3
  300.0 66.4 %all-gather.14.cloned.1.call-done = f32[128,64,128]{2,1,0:T(8,128)} async-done(((f32[16,64,128]{2,1,0:T(8,128)}), f32[128,64,128]{2,1,0:T(8,128)}) %all-gather.14.cloned.1.call-update) | async-done | bytes 4194320 | tf_op jit(solution)/shard_map/all_gather | solution.py:26
  366.5 13.5 %while.20 = (s32[]{:T(128)}, f32[16,64,128]{2,1,0:T(8,128)S(1)}, s32[]{:T(128)}, f32[8,16]{1,0:T(8,128)}, f32[8,16,64,128]{3,2,1,0:T(8,128)}, /*index=5*/s32[]{:T(128)}, s32[]{:T(128)}, s32[]{:T(128)}, s32[]{:T(128)}) while((s32[]{:T(128)}, f32[16,64,128]{2,1,0:T(8,128)S(1)}, s32[]{:T(128)}, f32[8,16]{1,0:T(8,128)}, ...), condition=%wide.region_13.14_spmd, body=%wide.region_12.13_spmd.sunk | while | flops 262150 | bytes 1573203 | solution.py:35
  367.2 1.2 bitcast_add_fusion.6
  369.1 1.2 bitcast_add_fusion.6
  371.0 1.2 bitcast_add_fusion.6
  372.9 1.2 bitcast_add_fusion.6
  374.8 1.2 bitcast_add_fusion.6
  376.7 1.2 bitcast_add_fusion.6
  378.6 1.2 bitcast_add_fusion.6
  380.1 1.0 convolution_bitcast_fusion.3
  381.1 1.3 bitcast_reduce_fusion.3
  384.0 2.0 reduce_window_sum.54
  386.0 2.6 reduce_window_sum.55
  388.6 1.5 add.137
  390.0 1.5 copy.272
  391.6 1.8 fusion.7
  393.3 1.7 copy.270
  395.0 1.1 fusion.3
  396.1 0.9 copy.268
  396.9 119.6 %reduce-scatter.5.cloned.1.call-done = f32[256,1024]{1,0:T(8,128)} async-done(((f32[2048,1024]{1,0:T(8,128)}), f32[256,1024]{1,0:T(8,128)}) %reduce-scatter.5.cloned.1.call-update) | async-done | bytes 1048592 | tf_op jit(solution)/shard_map/reduce_scatter | solution.py:210
  (178 shorter events, 21.9 us)
Async XLA Ops:
  8.0 39.1 %copy-start = (bf16[1,2048,256]{2,1,0:T(8,128)(2,1)S(1)}, bf16[1,2048,256]{2,1,0:T(8,128)(2,1)}, u32[]{:S(2)}) copy-start(bf16[1,2048,256]{2,1,0:T(8,128)(2,1)} %param.21) | copy-start | bytes 3145732
  8.0 39.1 %all-gather.8.cloned.1.call-start = ((), (), s32[]{:S(2)}) async-start(), calls=%async_computation.6 | async-start | bytes 1638400 | tf_op jit(solution)/shard_map/all_gather | solution.py:164
  30.3 36.5 %all-gather.10.cloned.1.call-start = ((), (), s32[]{:S(2)}) async-start(), calls=%async_computation.7 | async-start | bytes 1638400 | tf_op jit(solution)/shard_map/all_gather | solution.py:165
  46.2 2.8 copy-start.17
  46.3 52.3 %reduce-scatter.3.cloned.1.call-start = ((), (), s32[]{:S(2)}) async-start(), calls=%async_computation.8 | async-start | bytes 1638400 | tf_op jit(solution)/shard_map/reduce_scatter | solution.py:191
  47.1 1.9 copy-start.5
  49.1 20.0 %copy-start.31 = (f32[320,256]{1,0:T(8,128)}, f32[320,256]{1,0:T(8,128)S(1)}, u32[]{:S(2)}) copy-start(f32[320,256]{1,0:T(8,128)S(1)} %fusion.15) | copy-start | bytes 983044
  49.6 19.5 %copy-start.33 = (f32[320,256]{1,0:T(8,128)}, f32[320,256]{1,0:T(8,128)S(1)}, u32[]{:S(2)}) copy-start(f32[320,256]{1,0:T(8,128)S(1)} %fusion.18) | copy-start | bytes 983044
  69.1 0.7 copy-start.22
  69.1 1.2 copy-start.20
  70.3 1.7 copy-start.48
  70.3 2.1 copy-start.44
  71.9 0.9 copy-start.35
  72.0 160.7 %all-gather.12.cloned.1.call-start = ((), (), s32[]{:S(2)}) async-start(), calls=%async_computation.10 | async-start | bytes 4718592 | tf_op jit(solution)/shard_map/all_gather | solution.py:26
  72.3 153.0 %copy-start.15 = (f32[128,16]{1,0:T(8,128)}, f32[128,16]{1,0:T(8,128)S(1)}, u32[]{:S(2)}) copy-start(f32[128,16]{1,0:T(8,128)S(1)} %reduce_window_sum.53) | copy-start | bytes 24580
  72.3 2.8 copy-start.18
  72.4 2.8 copy-start.42
  73.0 31.0 %copy-start.27 = (bf16[256,1024]{1,0:T(8,128)(2,1)S(1)}, bf16[256,1024]{1,0:T(8,128)(2,1)}, u32[]{:S(2)}) copy-start(bf16[256,1024]{1,0:T(8,128)(2,1)} %param.24) | copy-start | bytes 1572868
  98.5 22.2 %all-to-all-start.2 = ((bf16[8,40,512]{2,1,0:T(8,128)(2,1)}), bf16[8,40,512]{2,1,0:T(8,128)(2,1)S(1)}, u32[]{:S(2)}, u32[]{:S(2)}) async-start(bf16[8,40,512]{2,1,0:T(8,128)(2,1)} %bitcast.246), calls=%async_computation.3 | async-start | bytes 655360 | tf_op jit(solution)/shard_map/all_to_all | solution.py:192
  122.9 4.8 copy-start.45
  122.9 6.8 %copy-start.36 = (bf16[128,1024]{1,0:T(8,128)(2,1)S(1)}, bf16[128,1024]{1,0:T(8,128)(2,1)}, u32[]{:S(2)}) copy-start(bf16[128,1024]{1,0:T(8,128)(2,1)} %param.29) | copy-start | bytes 786436
  123.0 119.4 %all-to-all-start.3 = ((bf16[8,256,1024]{1,2,0:T(8,128)(2,1)}), bf16[8,256,1024]{1,2,0:T(8,128)(2,1)}, u32[]{:S(2)}, u32[]{:S(2)}) async-start(bf16[8,256,1024]{1,2,0:T(8,128)(2,1)} %stack.11), calls=%async_computation.5 | async-start | bytes 8388608 | tf_op jit(solution)/shard_map/all_to_all | solution.py:19
  127.6 98.2 %copy-start.28 = (bf16[128,512]{1,0:T(8,128)(2,1)S(1)}, bf16[128,512]{1,0:T(8,128)(2,1)}, u32[]{:S(2)}) copy-start(bf16[128,512]{1,0:T(8,128)(2,1)} %param.18) | copy-start | bytes 393220
  127.7 238.8 %all-gather.14.cloned.1.call-start = ((), (), s32[]{:S(2)}) async-start(), calls=%async_computation.11 | async-start | bytes 4718592 | tf_op jit(solution)/shard_map/all_gather | solution.py:26
  128.6 104.1 %copy-start.24 = (bf16[128,2,128]{0,2,1:T(8,128)(2,1)}, bf16[128,2,128]{0,2,1:T(8,128)(2,1)S(1)}, u32[]{:S(2)}) copy-start(bf16[128,2,128]{0,2,1:T(8,128)(2,1)S(1)} %copy.259) | copy-start | bytes 196612
  128.7 0.6 copy-start.26
  129.7 96.1 %copy-start.13 = (f32[128,128,2]{1,0,2:T(8,128)}, f32[128,128,2]{1,0,2:T(8,128)S(1)}, u32[]{:S(2)}) copy-start(f32[128,128,2]{1,0,2:T(8,128)S(1)} %copy.238) | copy-start | bytes 393220
  130.6 95.2 %copy-start.40 = (pred[128,128]{1,0:T(8,128)(4,1)}, pred[128,128]{1,0:T(8,128)(4,1)S(1)}, u32[]{:S(2)}) copy-start(pred[128,128]{1,0:T(8,128)(4,1)S(1)} %iota_compare_fusion.2) | copy-start | bytes 49156
  232.7 22.7 %copy-start.4 = (bf16[128,2048]{1,0:T(8,128)(2,1)}, bf16[128,2048]{1,0:T(8,128)(2,1)S(1)}, u32[]{:S(2)}) copy-start(bf16[128,2048]{1,0:T(8,128)(2,1)S(1)} %all_gather.29) | copy-start | bytes 1572868
  232.9 0.6 copy-start.49
  233.5 3.2 copy-start.2
  234.6 4.2 copy-start.10
  236.8 3.6 copy-start.9
  238.0 0.8 copy-start.8
  255.4 4.0 copy-start.50
  255.4 4.6 copy-start.7
  259.4 0.6 copy-start.47
  265.6 250.9 %reduce-scatter.5.cloned.1.call-start = ((), (), s32[]{:S(2)}) async-start(), calls=%async_computation.9 | async-start | bytes 9437184 | tf_op jit(solution)/shard_map/reduce_scatter | solution.py:210
  272.5 1.9 copy-start.21
  272.6 1.8 copy-start.6
  274.4 2.1 copy-start.23
  276.5 2.1 copy-start.12
  276.5 2.1 copy-start.32
  276.5 2.1 copy-start.34
  278.6 2.1 copy-start.41
  280.7 1.9 copy-start.14
  280.7 4.0 copy-start.46
  285.4 11.7 %copy-start.3 = (f32[128,128,16]{1,0,2:T(8,128)S(1)}, f32[128,128,16]{1,0,2:T(8,128)}, u32[]{:S(2)}) copy-start(f32[128,128,16]{1,0,2:T(8,128)} %bitcast_multiply_fusion.4) | copy-start | bytes 3145732
  366.5 14.6 %copy-start.43 = (f32[128,16]{0,1:T(8,128)S(1)}, f32[128,16]{0,1:T(8,128)}, u32[]{:S(2)}) copy-start(f32[128,16]{0,1:T(8,128)} %copy-done.42) | copy-start | bytes 24580
  381.1 1.7 copy-start.19
  382.4 0.8 copy-start.16
  382.4 0.9 copy-start.37
  382.4 0.9 copy-start.38
  382.4 0.9 copy-start.39
  382.4 9.2 %copy-start.25 = (bf16[128,2,128]{0,2,1:T(8,128)(2,1)S(1)}, bf16[128,2,128]{0,2,1:T(8,128)(2,1)}, u32[]{:S(2)}) copy-start(bf16[128,2,128]{0,2,1:T(8,128)(2,1)} %copy-done.24) | copy-start | bytes 196612
  382.4 9.2 %copy-start.29 = (f32[128,128,2]{1,0,2:T(8,128)S(1)}, f32[128,128,2]{1,0,2:T(8,128)}, u32[]{:S(2)}) copy-start(f32[128,128,2]{1,0,2:T(8,128)} %get-tuple-element.541) | copy-start | bytes 393220
  382.6 9.0 %copy-start.30 = (f32[128,2,128]{0,2,1:T(8,128)S(1)}, f32[128,2,128]{0,2,1:T(8,128)}, u32[]{:S(2)}) copy-start(f32[128,2,128]{0,2,1:T(8,128)} %get-tuple-element.496) | copy-start | bytes 393220
  382.6 12.4 %copy-start.11 = (f32[16,64,128]{2,1,0:T(8,128)S(1)}, f32[16,64,128]{2,1,0:T(8,128)}, u32[]{:S(2)}) copy-start(f32[16,64,128]{2,1,0:T(8,128)} %convolution_add_fusion.3) | copy-start | bytes 1572868
  384.0 132.5 %copy-start.1 = (bf16[1,2048,256]{2,1,0:T(8,128)(2,1)S(1)}, bf16[1,2048,256]{2,1,0:T(8,128)(2,1)}, u32[]{:S(2)}) copy-start(bf16[1,2048,256]{2,1,0:T(8,128)(2,1)} %param.21) | copy-start | bytes 3145732
Sparse Core Ops, SparseCore 0:
  30.5 16.5 all-gather.7
  48.7 18.1 all-gather.9
  72.1 26.4 reduce-scatter.2
Sparse Core Ops, SparseCore 1:
  75.3 104.5 all-gather.11
  265.7 100.7 all-gather.13
  370.5 145.9 reduce-scatter.4
